TPU v7x, 32 devices: a whole 2x2x4 slice. The times are simulated.
32 devices in a mesh: grp: 2 (over y), fs: 4 (over z), tp: 4 (over x, core).
Axes of the slice: x: 2, y: 2, z: 4, core: 2. Of those that a mesh axis runs over, the one named last changes fastest.
Arguments:
- tokens: bfloat16 [2048, 2048], P(('grp', 'fs')), parts along dimension 0, may hold values from -6 to 6
- route_ids: int32 [2048, 2], P(('grp', 'fs')), parts along dimension 0, may hold values from 0 to 7, as said below
- route_weights: float32 [2048, 2], P(('grp', 'fs')), parts along dimension 0, may hold values from 0.2 to 1
- ffn_gain: float32 [2048], P('fs'), may hold values from 0.1 to 1.9
- gate_master: float32 [8, 2048, 1024], P(None, 'fs', 'tp'), may hold values from -0.125 to 0.125
- up_master: float32 [8, 2048, 1024], P(None, 'fs', 'tp'), may hold values from -0.125 to 0.125
- down_master: float32 [8, 1024, 2048], P(None, 'fs', 'tp'), may hold values from -0.1875 to 0.1875
Outputs:
- gate_serve: bfloat16 [16, 2048, 1024], P(('grp', 'fs'), None, 'tp'), parts along dimension 0
- up_serve: bfloat16 [16, 2048, 1024], P(('grp', 'fs'), None, 'tp'), parts along dimension 0
- down_serve: bfloat16 [16, 1024, 2048], P(('grp', 'fs'), None, 'tp'), parts along dimension 0
- mixed: bfloat16 [2048, 2048], P(('grp', 'fs'), 'tp'), parts along dimension 0
There are 2 independent parts, one for each index of `grp`. A program takes and returns all parts, laid end to end along the dimension named above; an argument that names none is the same for every part. Nothing has to cross between parts.
Inputs may be any that keep to these rules, and one draw needn't show every extreme that they name: `route_ids`: each row names two different experts of one group of 8 consecutive experts. Among the tokens of one index of fs, each group is named by exactly 256 tokens and no expert by more than 128; in every group one expert, the same for every index of fs, is named by exactly 128, and so is one other expert of the group, which may change from one index of fs to the next.
All inputs are finite; a program needn't handle non-finite values.
Results may differ from a plain program's by a relative error of at most 0.0087.
Values may be sent and summed in bfloat16 or wider, within the bound.
A program may use at most 64 MiB of HBM per device.

v0:
```python
import jax
import jax.numpy as jnp
from jax import lax
from jax.sharding import PartitionSpec as P

GROUP_SIZE = 8


def slot_targets(route_ids, experts, capacity):
    flat_ids = route_ids.reshape(-1)
    member = (flat_ids[:, None] == jnp.arange(experts, dtype=jnp.int32)[None, :]).astype(jnp.int32)
    before = jnp.cumsum(member, axis=0) - member
    slot_index = jnp.sum(before * member, axis=1)
    return flat_ids * capacity + slot_index


def fill_slots(source, targets, experts, capacity):
    doubled = jnp.repeat(source, 2, axis=0)
    buffer = jnp.zeros((experts * capacity, source.shape[1]), source.dtype).at[targets].set(doubled)
    return buffer.reshape(experts, capacity, source.shape[1])


def on_device(tokens, route_ids, route_weights, ffn_gain, gate_master, up_master, down_master):
    row_gain = ffn_gain[None, :, None]
    gate_local = (gate_master * row_gain).astype(jnp.bfloat16)
    up_local = (up_master * row_gain).astype(jnp.bfloat16)
    down_local = down_master.astype(jnp.bfloat16)
    gate_serve, up_serve, down_serve = (
        lax.all_to_all(gate_local, "fs", split_axis=0, concat_axis=1, tiled=True),
        lax.all_to_all(up_local, "fs", split_axis=0, concat_axis=1, tiled=True),
        lax.all_to_all(down_local, "fs", split_axis=0, concat_axis=1, tiled=True),
    )
    experts = gate_local.shape[0]
    capacity = tokens.shape[0] // (2 * (experts // GROUP_SIZE))
    token_rows = tokens.astype(jnp.float32)
    normed = (
        token_rows * lax.rsqrt(jnp.mean(token_rows * token_rows, axis=1, keepdims=True) + 1e-06)
    ).astype(jnp.bfloat16)
    targets = slot_targets(route_ids, experts, capacity)
    col_width = normed.shape[1] // lax.axis_size("tp")
    own_cols = lax.dynamic_slice_in_dim(normed, lax.axis_index("tp") * col_width, col_width, 1)
    part_rows = lax.all_to_all(
        fill_slots(own_cols, targets, experts, capacity),
        "fs",
        split_axis=0,
        concat_axis=1,
        tiled=True,
    )
    portion = lax.all_gather(part_rows, "tp", axis=2, tiled=True)
    gate_part = jnp.einsum("erd,edf->erf", portion, gate_serve, preferred_element_type=jnp.float32)
    up_part = jnp.einsum("erd,edf->erf", portion, up_serve, preferred_element_type=jnp.float32)
    hidden = (jax.nn.silu(gate_part) * up_part).astype(jnp.bfloat16)
    expert_out = jnp.einsum(
        "erf,efd->erd",
        lax.all_gather(hidden, "tp", axis=2, tiled=True),
        down_serve,
        preferred_element_type=jnp.float32,
    ).astype(jnp.bfloat16)
    returned_rows = lax.all_to_all(expert_out, "fs", split_axis=1, concat_axis=0, tiled=True)
    picked = returned_rows.reshape(-1, returned_rows.shape[2])[targets].astype(jnp.float32)
    weighted = picked * route_weights.reshape(-1, 1)
    combined = jnp.sum(weighted.reshape(-1, 2, returned_rows.shape[2]), axis=1).astype(jnp.bfloat16)
    return (gate_serve, up_serve, down_serve, combined)


def solution(mesh):
    in_specs = (
        P(("grp", "fs"), None),
        P(("grp", "fs"), None),
        P(("grp", "fs"), None),
        P("fs"),
        P(None, "fs", "tp"),
        P(None, "fs", "tp"),
        P(None, "fs", "tp"),
    )
    out_specs = (
        P(("grp", "fs"), None, "tp"),
        P(("grp", "fs"), None, "tp"),
        P(("grp", "fs"), None, "tp"),
        P(("grp", "fs"), "tp"),
    )
    return jax.shard_map(
        on_device, mesh=mesh, in_specs=in_specs, out_specs=out_specs, check_vma=False
    )
```

profile of v0, /device:TPU:0, one launch (start us, length us, event | category | flops | bytes accessed | tf_op | source)
XLA Modules:
  0.0 250.0 jit_solution(12472034540438758420)
XLA Ops:
  7.2 0.0 copy-start
  7.2 1.5 convert_element_type.43
  8.7 0.3 multiply_reduce_fusion
  9.0 0.0 copy-done.2
  9.0 0.1 copy.29
  9.2 0.1 eq.29
  9.3 0.1 eq.25
  9.5 0.1 fusion.1
  9.6 0.3 broadcast_in_dim.5
  9.9 0.0 copy-start.4
  9.9 0.2 reshape.101
  10.1 1.1 reduce-window.6
  11.3 0.2 slice_reduce_fusion
  11.5 0.1 copy.28
  11.7 0.1 mul.68
  11.8 0.1 fusion.5
  11.9 3.5 %scatter_custom_fusion = bf16[1024,512]{1,0:T(8,128)(2,1)} fusion(s32[512]{0:T(512)S(1)} %bitcast.49, bf16[512,512]{1,0:T(8,128)(2,1)S(1)} %reshape.101, bf16[]{:T(256)} %constant.11.clone.1), kind=kCustom, calls=%fused_computation.11 | custom fusion | bytes 1048578 | tf_op jit(solution)/shard_map/scatter | solution.py:19
  15.4 6.3 %all-to-all-start.3 = ((bf16[8,128,512]{2,1,0:T(8,128)(2,1)}), bf16[8,128,512]{2,1,0:T(8,128)(2,1)S(1)}, u32[]{:S(2)}, u32[]{:S(2)}) async-start(bf16[8,128,512]{2,1,0:T(8,128)(2,1)} %bitcast.13), calls=%async_computation.3 | async-start | bytes 2097152 | tf_op jit(solution)/shard_map/all_to_all | solution.py:42
  21.7 6.5 %multiply_convert_fusion = (bf16[8,512,256]{2,1,0:T(8,128)(2,1)}, bf16[8,512,256]{2,1,0:T(8,128)(2,1)}) fusion(f32[8,512,256]{2,1,0:T(8,128)} %param.12, f32[512]{0:T(512)S(1)} %copy-done.4, f32[8,512,256]{2,1,0:T(8,128)} %param.11), kind=kLoop, calls=%fused_computation.2 | loop fusion | flops 4194304 | bytes 12584960 | tf_op jit(solution)/shard_map/convert_element_type | solution.py:26
  28.2 19.3 %all-to-all-done.3 = bf16[8,128,512]{2,1,0:T(8,128)(2,1)S(1)} async-done(((bf16[8,128,512]{2,1,0:T(8,128)(2,1)}), bf16[8,128,512]{2,1,0:T(8,128)(2,1)S(1)}, u32[]{:S(2)}, u32[]{:S(2)}) %all-to-all-start.3) | async-done | bytes 1048608 | tf_op jit(solution)/shard_map/all_to_all | solution.py:42
  47.5 3.6 %all-to-all-start = ((bf16[8,512,256]{2,1,0:T(8,128)(2,1)}), bf16[8,512,256]{2,1,0:T(8,128)(2,1)S(1)}, u32[]{:S(2)}, u32[]{:S(2)}) async-start(bf16[8,512,256]{2,1,0:T(8,128)(2,1)} %get-tuple-element.5), calls=%async_computation | async-start | bytes 4194304 | tf_op jit(solution)/shard_map/all_to_all | solution.py:29
  51.1 0.0 all-gather.3.cloned.1.call-start
  51.1 1.2 copy.31
  52.3 0.0 all-gather.3.cloned.1.call-update
  52.3 46.5 %all-to-all-done = bf16[8,512,256]{2,1,0:T(8,128)(2,1)S(1)} async-done(((bf16[8,512,256]{2,1,0:T(8,128)(2,1)}), bf16[8,512,256]{2,1,0:T(8,128)(2,1)S(1)}, u32[]{:S(2)}, u32[]{:S(2)}) %all-to-all-start) | async-done | bytes 2097184 | tf_op jit(solution)/shard_map/all_to_all | solution.py:29
  98.8 4.5 %all-to-all-start.1 = ((bf16[8,512,256]{2,1,0:T(8,128)(2,1)}), bf16[8,512,256]{2,1,0:T(8,128)(2,1)}, u32[]{:S(2)}, u32[]{:S(2)}) async-start(bf16[8,512,256]{2,1,0:T(8,128)(2,1)} %get-tuple-element.4), calls=%async_computation.1 | async-start | bytes 4194304 | tf_op jit(solution)/shard_map/all_to_all | solution.py:30
  103.3 3.8 %convert_element_type.40 = bf16[8,256,512]{2,1,0:T(8,128)(2,1)} convert(f32[8,256,512]{2,1,0:T(8,128)} %param.13) | non-fusion elementwise | flops 1048576 | bytes 6291456 | tf_op jit(solution)/shard_map/convert_element_type | solution.py:27
  107.0 1.5 copy.25
  108.5 42.6 %all-to-all-done.1 = bf16[8,512,256]{2,1,0:T(8,128)(2,1)} async-done(((bf16[8,512,256]{2,1,0:T(8,128)(2,1)}), bf16[8,512,256]{2,1,0:T(8,128)(2,1)}, u32[]{:S(2)}, u32[]{:S(2)}) %all-to-all-start.1) | async-done | bytes 2097184 | tf_op jit(solution)/shard_map/all_to_all | solution.py:30
  151.1 3.6 %all-to-all-start.2 = ((bf16[8,256,512]{2,1,0:T(8,128)(2,1)}), bf16[8,256,512]{2,1,0:T(8,128)(2,1)S(1)}, u32[]{:S(2)}, u32[]{:S(2)}) async-start(bf16[8,256,512]{2,1,0:T(8,128)(2,1)} %convert_element_type.40), calls=%async_computation.2 | async-start | bytes 4194304 | tf_op jit(solution)/shard_map/all_to_all | solution.py:31
  154.7 0.0 all-gather.5.cloned.1.call-start
  154.7 3.0 %copy.26 = bf16[4,2,512,256]{3,2,0,1:T(8,128)(2,1)} copy(bf16[4,2,512,256]{3,2,1,0:T(8,128)(2,1)} %bitcast.3) | data formatting | bytes 4194304 | tf_op jit(solution)/shard_map/all_to_all | solution.py:30
  157.8 4.2 %fusion.7 = f32[2,512,256]{2,1,0:T(8,128)S(1)} fusion(bf16[2,512,2048]{2,1,0:T(8,128)(2,1)} %all-gather.3.cloned.1.call-done, bf16[2,2048,256]{2,1,0:T(8,128)(2,1)} %bitcast.43), kind=kOutput, calls=%fused_computation.24 | convolution fusion | flops 1073741824 | bytes 7340032 | tf_op jit(solution)/shard_map/erd,edf->erf/dot_general | solution.py:50
  162.1 0.4 copy-done.5
  162.5 2.1 fusion
  164.6 0.0 all-gather.5.cloned.1.call-update
  164.6 37.8 %all-to-all-done.2 = bf16[8,256,512]{2,1,0:T(8,128)(2,1)S(1)} async-done(((bf16[8,256,512]{2,1,0:T(8,128)(2,1)}), bf16[8,256,512]{2,1,0:T(8,128)(2,1)S(1)}, u32[]{:S(2)}, u32[]{:S(2)}) %all-to-all-start.2) | async-done | bytes 2097184 | tf_op jit(solution)/shard_map/all_to_all | solution.py:31
  202.4 1.5 copy.27
  204.0 3.5 %convolution_convert_fusion = bf16[2,512,512]{2,1,0:T(8,128)(2,1)S(1)} fusion(bf16[2,512,1024]{2,1,0:T(8,128)(2,1)} %all-gather.5.cloned.1.call-done, bf16[2,1024,512]{2,1,0:T(8,128)(2,1)} %bitcast.47), kind=kOutput, calls=%fused_computation.5 | convolution fusion | flops 1074266112 | bytes 5242880 | tf_op jit(solution)/shard_map/erf,efd->erd/dot_general | solution.py:53
  207.4 0.0 copy-start.3
  207.4 2.0 copy.32
  209.5 3.7 %all-to-all-start.4 = ((bf16[2,512,512]{2,0,1:T(2,128)(2,1)}), bf16[2,512,512]{2,0,1:T(2,128)(2,1)S(1)}, u32[]{:S(2)}, u32[]{:S(2)}) async-start(bf16[2,512,512]{2,0,1:T(2,128)(2,1)} %copy.32), calls=%async_computation.4 | async-start | bytes 2097152 | tf_op jit(solution)/shard_map/all_to_all | solution.py:59
  213.2 0.1 copy.34
  213.4 24.9 %all-to-all-done.4 = bf16[2,512,512]{2,0,1:T(2,128)(2,1)S(1)} async-done(((bf16[2,512,512]{2,0,1:T(2,128)(2,1)}), bf16[2,512,512]{2,0,1:T(2,128)(2,1)S(1)}, u32[]{:S(2)}, u32[]{:S(2)}) %all-to-all-start.4) | async-done | bytes 1048608 | tf_op jit(solution)/shard_map/all_to_all | solution.py:59
  238.3 0.2 copy.33
  238.4 2.0 gather_fusion
  240.4 0.7 reshape.88
  241.1 2.1 multiply_reduce_fusion.1
  (16 shorter events, 0.1 us)
Async XLA Ops:
  7.2 1.6 copy-start
  7.2 1.9 copy-start.2
  9.9 11.8 %copy-start.4 = (f32[512]{0:T(512)S(1)}, f32[512]{0:T(512)}, u32[]{:S(2)}) copy-start(f32[512]{0:T(512)} %param.10) | copy-start | bytes 6148
  15.4 32.1 %all-to-all-start.3 = ((bf16[8,128,512]{2,1,0:T(8,128)(2,1)}), bf16[8,128,512]{2,1,0:T(8,128)(2,1)S(1)}, u32[]{:S(2)}, u32[]{:S(2)}) async-start(bf16[8,128,512]{2,1,0:T(8,128)(2,1)} %bitcast.13), calls=%async_computation.3 | async-start | bytes 2097152 | tf_op jit(solution)/shard_map/all_to_all | solution.py:42
  47.5 51.3 %all-to-all-start = ((bf16[8,512,256]{2,1,0:T(8,128)(2,1)}), bf16[8,512,256]{2,1,0:T(8,128)(2,1)S(1)}, u32[]{:S(2)}, u32[]{:S(2)}) async-start(bf16[8,512,256]{2,1,0:T(8,128)(2,1)} %get-tuple-element.5), calls=%async_computation | async-start | bytes 4194304 | tf_op jit(solution)/shard_map/all_to_all | solution.py:29
  51.1 106.7 %all-gather.3.cloned.1.call-start = ((), (), s32[]{:S(2)}) async-start(), calls=%async_computation.5 | async-start | bytes 5242880 | tf_op jit(solution)/shard_map/all_gather | solution.py:49
  98.8 52.3 %all-to-all-start.1 = ((bf16[8,512,256]{2,1,0:T(8,128)(2,1)}), bf16[8,512,256]{2,1,0:T(8,128)(2,1)}, u32[]{:S(2)}, u32[]{:S(2)}) async-start(bf16[8,512,256]{2,1,0:T(8,128)(2,1)} %get-tuple-element.4), calls=%async_computation.1 | async-start | bytes 4194304 | tf_op jit(solution)/shard_map/all_to_all | solution.py:30
  151.1 51.3 %all-to-all-start.2 = ((bf16[8,256,512]{2,1,0:T(8,128)(2,1)}), bf16[8,256,512]{2,1,0:T(8,128)(2,1)S(1)}, u32[]{:S(2)}, u32[]{:S(2)}) async-start(bf16[8,256,512]{2,1,0:T(8,128)(2,1)} %convert_element_type.40), calls=%async_computation.2 | async-start | bytes 4194304 | tf_op jit(solution)/shard_map/all_to_all | solution.py:31
  154.7 49.3 %all-gather.5.cloned.1.call-start = ((), (), s32[]{:S(2)}) async-start(), calls=%async_computation.6 | async-start | bytes 2621440 | tf_op jit(solution)/shard_map/all_gather | solution.py:55
  157.8 4.3 %copy-start.1 = (bf16[4,2,512,256]{3,2,0,1:T(8,128)(2,1)S(1)}, bf16[4,2,512,256]{3,2,0,1:T(8,128)(2,1)}, u32[]{:S(2)}) copy-start(bf16[4,2,512,256]{3,2,0,1:T(8,128)(2,1)} %copy.26) | copy-start | bytes 6291460
  157.8 4.7 %copy-start.5 = (bf16[2,512,2048]{2,1,0:T(8,128)(2,1)S(1)}, bf16[2,512,2048]{2,1,0:T(8,128)(2,1)}, u32[]{:S(2)}) copy-start(bf16[2,512,2048]{2,1,0:T(8,128)(2,1)} %all-gather.3.cloned.1.call-done) | copy-start | bytes 12582916
  207.4 5.8 %copy-start.3 = (f32[256,2]{0,1:T(2,128)S(1)}, f32[256,2]{0,1:T(2,128)}, u32[]{:S(2)}) copy-start(f32[256,2]{0,1:T(2,128)} %param.9) | copy-start | bytes 6148
  209.5 28.8 %all-to-all-start.4 = ((bf16[2,512,512]{2,0,1:T(2,128)(2,1)}), bf16[2,512,512]{2,0,1:T(2,128)(2,1)S(1)}, u32[]{:S(2)}, u32[]{:S(2)}) async-start(bf16[2,512,512]{2,0,1:T(2,128)(2,1)} %copy.32), calls=%async_computation.4 | async-start | bytes 2097152 | tf_op jit(solution)/shard_map/all_to_all | solution.py:59
Sparse Core Ops, SparseCore 0:
  53.5 35.8 all-gather.2
  164.8 24.1 all-gather.4
where the time goes:
time: 251 us; the launch traced here: 250 us
  waiting for transfers between devices  171 us (68%)
  starting transfers between devices  21.8 us (9%)
  local copies, waits for them, and re-layouts  17.5 us (7%)
  other arithmetic  15.5 us (6%)
  between operations  14.3 us (6%)
  matrix products  9.85 us (4%)
    all_to_all x1, waiting for transfers between devices, on_device(): lax.all_to_all(gate_local, 'fs', split_axis=0, concat_axis=1, tiled=True)  46.5 us
    all_to_all x1, waiting for transfers between devices, on_device(): lax.all_to_all(up_local, 'fs', split_axis=0, concat_axis=1, tiled=True)  42.6 us
    all_to_all x1, waiting for transfers between devices, on_device(): lax.all_to_all(down_local, 'fs', split_axis=0, concat_axis=1, tiled=True)  37.8 us
    all_to_all x1, waiting for transfers between devices, on_device(): lax.all_to_all(expert_out, 'fs', split_axis=1, concat_axis=0, tiled=True)  24.9 us
    all_to_all x1, waiting for transfers between devices, on_device(): lax.all_to_all(fill_slots(own_cols, targets, experts, capacity), 'fs', sp...  19.3 us
    convert_element_type x1, other arithmetic, on_device(): up_local = (up_master * row_gain).astype(jnp.bfloat16)  6.46 us
    all_to_all x1, starting transfers between devices, on_device(): lax.all_to_all(fill_slots(own_cols, targets, experts, capacity), 'fs', sp...  6.35 us
  transfers between devices with their start and end apart: 7, of which 5 were waited for; matrix products, arithmetic and copies ran while one was open for 10% of the time, Pallas kernels for 0%

commit v1 on v0

--- a/solution.py
+++ b/solution.py
@@ -4,6 +4,18 @@
 from jax.sharding import PartitionSpec as P
 
 GROUP_SIZE = 8
+
+
+def rotated_exchange(value, axis, split, join):
+    ways, here = (lax.axis_size(axis), lax.axis_index(axis))
+    width = value.shape[split] // ways
+    turned = jnp.roll(value, -here * width, axis=split)
+    got = [lax.slice_in_dim(turned, 0, width, axis=split)]
+    for far in range(1, ways):
+        sent = lax.slice_in_dim(turned, far * width, (far + 1) * width, axis=split)
+        got.append(lax.ppermute(sent, axis, [(d, (d + far) % ways) for d in range(ways)]))
+    line = jnp.concatenate(got[::-1], axis=join)
+    return jnp.roll(line, (here + 1) * got[0].shape[join], axis=join)
 
 
 def slot_targets(route_ids, experts, capacity):
@@ -39,13 +51,7 @@
     targets = slot_targets(route_ids, experts, capacity)
     col_width = normed.shape[1] // lax.axis_size("tp")
     own_cols = lax.dynamic_slice_in_dim(normed, lax.axis_index("tp") * col_width, col_width, 1)
-    part_rows = lax.all_to_all(
-        fill_slots(own_cols, targets, experts, capacity),
-        "fs",
-        split_axis=0,
-        concat_axis=1,
-        tiled=True,
-    )
+    part_rows = rotated_exchange(fill_slots(own_cols, targets, experts, capacity), "fs", 0, 1)
     portion = lax.all_gather(part_rows, "tp", axis=2, tiled=True)
     gate_part = jnp.einsum("erd,edf->erf", portion, gate_serve, preferred_element_type=jnp.float32)
     up_part = jnp.einsum("erd,edf->erf", portion, up_serve, preferred_element_type=jnp.float32)

time: 251 us -> 241 us (0.960)
  waiting for transfers between devices: 171 us -> 156 us
  local copies, waits for them, and re-layouts: 17.5 us -> 21.6 us
    ppermute x0 -> x3, waiting for transfers between devices: none -> 23.4 us  [rotated_exchange(): lax.ppermute(sent, axis, [(d, (d + far) % ways) for d in range(ways)])]
    all_to_all x1 -> x0, waiting for transfers between devices: 19.3 us -> none  [on_device(): lax.all_to_all(fill_slots(own_cols, targets, experts, capacity), 'fs', sp...]
    all_to_all x1, waiting for transfers between devices: 46.5 us -> 27.4 us  [on_device(): lax.all_to_all(gate_local, 'fs', split_axis=0, concat_axis=1, tiled=True)]
    all_to_all x1 -> x0, starting transfers between devices: 6.35 us -> none  [on_device(): lax.all_to_all(fill_slots(own_cols, targets, experts, capacity), 'fs', sp...]
    ppermute x0 -> x3, starting transfers between devices: none -> 6.09 us  [rotated_exchange(): lax.ppermute(sent, axis, [(d, (d + far) % ways) for d in range(ways)])]
    unnamed x14 -> x21, local copies, waits for them, and re-layouts: 0.71 us -> 4.65 us
  transfers between devices with their start and end apart: 7 -> 9, of which waited for: 5 -> 5; matrix products, arithmetic and copies ran while one was open for 10% -> 12% of each run, Pallas kernels for 0% -> 0%
where the time goes in v1:
time: 241 us; the launch traced here: 240 us
  waiting for transfers between devices  156 us (65%)
  starting transfers between devices  22.5 us (9%)
  local copies, waits for them, and re-layouts  21.6 us (9%)
  other arithmetic  15.9 us (7%)
  between operations  14.4 us (6%)
  matrix products  9.85 us (4%)
    all_to_all x1, waiting for transfers between devices, on_device(): lax.all_to_all(up_local, 'fs', split_axis=0, concat_axis=1, tiled=True)  42.5 us
    all_to_all x1, waiting for transfers between devices, on_device(): lax.all_to_all(down_local, 'fs', split_axis=0, concat_axis=1, tiled=True)  37.8 us
    all_to_all x1, waiting for transfers between devices, on_device(): lax.all_to_all(gate_local, 'fs', split_axis=0, concat_axis=1, tiled=True)  27.4 us
    all_to_all x1, waiting for transfers between devices, on_device(): lax.all_to_all(expert_out, 'fs', split_axis=1, concat_axis=0, tiled=True)  24.9 us
    ppermute x3, waiting for transfers between devices, rotated_exchange(): lax.ppermute(sent, axis, [(d, (d + far) % ways) for d in range(ways)])  23.4 us
    convert_element_type x1, other arithmetic, on_device(): up_local = (up_master * row_gain).astype(jnp.bfloat16)  6.46 us
    ppermute x3, starting transfers between devices, rotated_exchange(): lax.ppermute(sent, axis, [(d, (d + far) % ways) for d in range(ways)])  6.09 us
    all_to_all x1, starting transfers between devices, on_device(): lax.all_to_all(up_local, 'fs', split_axis=0, concat_axis=1, tiled=True)  4.98 us
  transfers between devices with their start and end apart: 9, of which 5 were waited for; matrix products, arithmetic and copies ran while one was open for 12% of the time, Pallas kernels for 0%

profile of v1, /device:TPU:0, one launch (start us, length us, event | category | flops | bytes accessed | tf_op | source)
XLA Modules:
  0.0 240.2 jit_solution(710598974531113740)
XLA Ops:
  7.2 1.5 convert_element_type.43
  8.8 0.3 multiply_reduce_fusion
  9.1 0.1 copy.28
  9.2 0.1 eq.34
  9.3 0.1 eq.30
  9.5 0.1 fusion.2
  9.6 0.3 broadcast_in_dim.5
  9.9 0.2 reshape.101
  10.1 1.1 reduce-window.6
  11.3 0.2 slice_reduce_fusion
  11.5 0.1 copy.27
  11.7 0.1 mul.74
  11.8 0.1 fusion.6
  11.9 2.7 %scatter_custom_fusion = bf16[1024,512]{1,0:T(8,128)(2,1)S(1)} fusion(s32[512]{0:T(512)S(1)} %bitcast.44, bf16[512,512]{1,0:T(8,128)(2,1)S(1)} %reshape.101, bf16[]{:T(256)} %constant.59.clone.1), kind=kCustom, calls=%fused_computation.14 | custom fusion | bytes 1048578 | tf_op jit(solution)/shard_map/scatter | solution.py:31
  14.7 0.4 fusion.1
  15.1 0.9 fusion.8
  16.0 5.1 %collective-permute-start = (bf16[2,128,512]{2,1,0:T(8,128)(2,1)}, bf16[2,128,512]{2,1,0:T(8,128)(2,1)S(1)}, u32[]{:S(2)}, u32[]{:S(2)}) collective-permute-start(bf16[2,128,512]{2,1,0:T(8,128)(2,1)} %get-tuple-element.6), channel_id=1, source_target_pairs={{0,12},{4,0},{8,4},{12,8},{1,13},{5,1},{9,5},{13,9},{2,14},{6,2},{... | collective-permute-start | bytes 786440 | tf_op jit(solution)/shard_map/ppermute | solution.py:16
  21.1 1.0 collective-permute-start.2
  22.1 6.5 %multiply_convert_fusion = (bf16[8,512,256]{2,1,0:T(8,128)(2,1)}, bf16[8,512,256]{2,1,0:T(8,128)(2,1)}) fusion(f32[8,512,256]{2,1,0:T(8,128)} %param.12, f32[512]{0:T(512)S(1)} %copy-done.4, f32[8,512,256]{2,1,0:T(8,128)} %param.11), kind=kLoop, calls=%fused_computation.2 | loop fusion | flops 4194304 | bytes 12584960 | tf_op jit(solution)/shard_map/convert_element_type | solution.py:38
  28.5 4.1 %all-to-all-start = ((bf16[8,512,256]{2,1,0:T(8,128)(2,1)}), bf16[8,512,256]{2,1,0:T(8,128)(2,1)S(1)}, u32[]{:S(2)}, u32[]{:S(2)}) async-start(bf16[8,512,256]{2,1,0:T(8,128)(2,1)} %get-tuple-element.8), calls=%async_computation | async-start | bytes 4194304 | tf_op jit(solution)/shard_map/all_to_all | solution.py:41
  32.7 23.4 %collective-permute-done.1 = bf16[2,128,512]{2,1,0:T(8,128)(2,1)} collective-permute-done((bf16[2,128,512]{2,1,0:T(8,128)(2,1)}, bf16[2,128,512]{2,1,0:T(8,128)(2,1)}, u32[]{:S(2)}, u32[]{:S(2)}) %collective-permute-start.1) | collective-permute-done | bytes 262176 | tf_op jit(solution)/shard_map/ppermute | solution.py:16
  56.1 1.0 constant_dynamic-update-slice_fusion.4
  57.1 1.0 constant_dynamic-update-slice_fusion.3
  58.1 1.0 constant_dynamic-update-slice_fusion.1
  59.1 1.0 constant_dynamic-update-slice_fusion
  60.1 1.1 constant_dynamic-slice_fusion
  61.2 27.4 %all-to-all-done = bf16[8,512,256]{2,1,0:T(8,128)(2,1)S(1)} async-done(((bf16[8,512,256]{2,1,0:T(8,128)(2,1)}), bf16[8,512,256]{2,1,0:T(8,128)(2,1)S(1)}, u32[]{:S(2)}, u32[]{:S(2)}) %all-to-all-start) | async-done | bytes 2097184 | tf_op jit(solution)/shard_map/all_to_all | solution.py:41
  88.6 5.0 %all-to-all-start.1 = ((bf16[8,512,256]{2,1,0:T(8,128)(2,1)}), bf16[8,512,256]{2,1,0:T(8,128)(2,1)}, u32[]{:S(2)}, u32[]{:S(2)}) async-start(bf16[8,512,256]{2,1,0:T(8,128)(2,1)} %get-tuple-element.7), calls=%async_computation.1 | async-start | bytes 4194304 | tf_op jit(solution)/shard_map/all_to_all | solution.py:42
  93.5 3.8 %convert_element_type.40 = bf16[8,256,512]{2,1,0:T(8,128)(2,1)} convert(f32[8,256,512]{2,1,0:T(8,128)} %param.13) | non-fusion elementwise | flops 1048576 | bytes 6291456 | tf_op jit(solution)/shard_map/convert_element_type | solution.py:39
  97.3 1.5 copy.24
  98.8 42.5 %all-to-all-done.1 = bf16[8,512,256]{2,1,0:T(8,128)(2,1)} async-done(((bf16[8,512,256]{2,1,0:T(8,128)(2,1)}), bf16[8,512,256]{2,1,0:T(8,128)(2,1)}, u32[]{:S(2)}, u32[]{:S(2)}) %all-to-all-start.1) | async-done | bytes 2097184 | tf_op jit(solution)/shard_map/all_to_all | solution.py:42
  141.3 3.6 %all-to-all-start.2 = ((bf16[8,256,512]{2,1,0:T(8,128)(2,1)}), bf16[8,256,512]{2,1,0:T(8,128)(2,1)S(1)}, u32[]{:S(2)}, u32[]{:S(2)}) async-start(bf16[8,256,512]{2,1,0:T(8,128)(2,1)} %convert_element_type.40), calls=%async_computation.2 | async-start | bytes 4194304 | tf_op jit(solution)/shard_map/all_to_all | solution.py:43
  144.9 0.0 all-gather.5.cloned.1.call-start
  145.0 3.0 %copy.25 = bf16[4,2,512,256]{3,2,0,1:T(8,128)(2,1)} copy(bf16[4,2,512,256]{3,2,1,0:T(8,128)(2,1)} %bitcast.3) | data formatting | bytes 4194304 | tf_op jit(solution)/shard_map/all_to_all | solution.py:42
  148.0 4.2 %fusion.9 = f32[2,512,256]{2,1,0:T(8,128)S(1)} fusion(bf16[2,512,2048]{2,1,0:T(8,128)(2,1)} %all-gather.3.cloned.1.call-done, bf16[2,2048,256]{2,1,0:T(8,128)(2,1)} %bitcast.38), kind=kOutput, calls=%fused_computation.37 | convolution fusion | flops 1073741824 | bytes 7340032 | tf_op jit(solution)/shard_map/erd,edf->erf/dot_general | solution.py:56
  152.3 0.4 copy-done.5
  152.7 2.1 fusion
  154.9 37.8 %all-to-all-done.2 = bf16[8,256,512]{2,1,0:T(8,128)(2,1)S(1)} async-done(((bf16[8,256,512]{2,1,0:T(8,128)(2,1)}), bf16[8,256,512]{2,1,0:T(8,128)(2,1)S(1)}, u32[]{:S(2)}, u32[]{:S(2)}) %all-to-all-start.2) | async-done | bytes 2097184 | tf_op jit(solution)/shard_map/all_to_all | solution.py:43
  192.6 1.5 copy.26
  194.2 3.5 %convolution_convert_fusion = bf16[2,512,512]{2,1,0:T(8,128)(2,1)S(1)} fusion(bf16[2,512,1024]{2,1,0:T(8,128)(2,1)} %all-gather.5.cloned.1.call-done, bf16[2,1024,512]{2,1,0:T(8,128)(2,1)} %bitcast.42), kind=kOutput, calls=%fused_computation.7 | convolution fusion | flops 1074266112 | bytes 5242880 | tf_op jit(solution)/shard_map/erf,efd->erd/dot_general | solution.py:59
  197.7 2.1 copy.30
  199.7 3.7 %all-to-all-start.3 = ((bf16[2,512,512]{2,0,1:T(2,128)(2,1)}), bf16[2,512,512]{2,0,1:T(2,128)(2,1)S(1)}, u32[]{:S(2)}, u32[]{:S(2)}) async-start(bf16[2,512,512]{2,0,1:T(2,128)(2,1)} %copy.30), calls=%async_computation.3 | async-start | bytes 2097152 | tf_op jit(solution)/shard_map/all_to_all | solution.py:65
  203.4 0.1 copy.32
  203.6 24.9 %all-to-all-done.3 = bf16[2,512,512]{2,0,1:T(2,128)(2,1)S(1)} async-done(((bf16[2,512,512]{2,0,1:T(2,128)(2,1)}), bf16[2,512,512]{2,0,1:T(2,128)(2,1)S(1)}, u32[]{:S(2)}, u32[]{:S(2)}) %all-to-all-start.3) | async-done | bytes 1048608 | tf_op jit(solution)/shard_map/all_to_all | solution.py:65
  228.5 0.2 copy.31
  228.7 2.0 gather_fusion
  230.7 0.7 reshape.88
  231.3 2.1 multiply_reduce_fusion.1
  (30 shorter events, 0.2 us)
Async XLA Ops:
  7.2 1.6 copy-start
  7.2 1.9 copy-start.2
  14.7 7.4 %copy-start.4 = (f32[512]{0:T(512)S(1)}, f32[512]{0:T(512)}, u32[]{:S(2)}) copy-start(f32[512]{0:T(512)} %param.10) | copy-start | bytes 6148
  16.0 16.6 %collective-permute-start = (bf16[2,128,512]{2,1,0:T(8,128)(2,1)}, bf16[2,128,512]{2,1,0:T(8,128)(2,1)S(1)}, u32[]{:S(2)}, u32[]{:S(2)}) collective-permute-start(bf16[2,128,512]{2,1,0:T(8,128)(2,1)} %get-tuple-element.6), channel_id=1, source_target_pairs={{0,12},{4,0},{8,4},{12,8},{1,13},{5,1},{9,5},{13,9},{2,14},{6,2},{... | collective-permute-start | bytes 786440 | tf_op jit(solution)/shard_map/ppermute | solution.py:16
  21.1 35.0 %collective-permute-start.1 = (bf16[2,128,512]{2,1,0:T(8,128)(2,1)}, bf16[2,128,512]{2,1,0:T(8,128)(2,1)}, u32[]{:S(2)}, u32[]{:S(2)}) collective-permute-start(bf16[2,128,512]{2,1,0:T(8,128)(2,1)} %get-tuple-element.5), channel_id=1, source_target_pairs={{0,8},{4,12},{8,0},{12,4},{1,9},{5,13},{9,1},{13,5},{2,10},{6,14},... | collective-permute-start | bytes 786440 | tf_op jit(solution)/shard_map/ppermute | solution.py:16
  21.1 36.0 %collective-permute-start.2 = (bf16[2,128,512]{2,1,0:T(8,128)(2,1)}, bf16[2,128,512]{2,1,0:T(8,128)(2,1)}, u32[]{:S(2)}, u32[]{:S(2)}) collective-permute-start(bf16[2,128,512]{2,1,0:T(8,128)(2,1)} %get-tuple-element.4), channel_id=1, source_target_pairs={{0,4},{4,8},{8,12},{12,0},{1,5},{5,9},{9,13},{13,1},{2,6},{6,10},{... | collective-permute-start | bytes 786440 | tf_op jit(solution)/shard_map/ppermute | solution.py:16
  28.5 60.0 %all-to-all-start = ((bf16[8,512,256]{2,1,0:T(8,128)(2,1)}), bf16[8,512,256]{2,1,0:T(8,128)(2,1)S(1)}, u32[]{:S(2)}, u32[]{:S(2)}) async-start(bf16[8,512,256]{2,1,0:T(8,128)(2,1)} %get-tuple-element.8), calls=%async_computation | async-start | bytes 4194304 | tf_op jit(solution)/shard_map/all_to_all | solution.py:41
  32.6 115.4 %all-gather.3.cloned.1.call-start = ((), (), s32[]{:S(2)}) async-start(), calls=%async_computation.4 | async-start | bytes 5242880 | tf_op jit(solution)/shard_map/all_gather | solution.py:55
  88.6 52.7 %all-to-all-start.1 = ((bf16[8,512,256]{2,1,0:T(8,128)(2,1)}), bf16[8,512,256]{2,1,0:T(8,128)(2,1)}, u32[]{:S(2)}, u32[]{:S(2)}) async-start(bf16[8,512,256]{2,1,0:T(8,128)(2,1)} %get-tuple-element.7), calls=%async_computation.1 | async-start | bytes 4194304 | tf_op jit(solution)/shard_map/all_to_all | solution.py:42
  141.3 51.3 %all-to-all-start.2 = ((bf16[8,256,512]{2,1,0:T(8,128)(2,1)}), bf16[8,256,512]{2,1,0:T(8,128)(2,1)S(1)}, u32[]{:S(2)}, u32[]{:S(2)}) async-start(bf16[8,256,512]{2,1,0:T(8,128)(2,1)} %convert_element_type.40), calls=%async_computation.2 | async-start | bytes 4194304 | tf_op jit(solution)/shard_map/all_to_all | solution.py:43
  144.9 49.3 %all-gather.5.cloned.1.call-start = ((), (), s32[]{:S(2)}) async-start(), calls=%async_computation.5 | async-start | bytes 2621440 | tf_op jit(solution)/shard_map/all_gather | solution.py:61
  148.0 4.3 %copy-start.1 = (bf16[4,2,512,256]{3,2,0,1:T(8,128)(2,1)S(1)}, bf16[4,2,512,256]{3,2,0,1:T(8,128)(2,1)}, u32[]{:S(2)}) copy-start(bf16[4,2,512,256]{3,2,0,1:T(8,128)(2,1)} %copy.25) | copy-start | bytes 6291460
  148.0 4.7 %copy-start.5 = (bf16[2,512,2048]{2,1,0:T(8,128)(2,1)S(1)}, bf16[2,512,2048]{2,1,0:T(8,128)(2,1)}, u32[]{:S(2)}) copy-start(bf16[2,512,2048]{2,1,0:T(8,128)(2,1)} %all-gather.3.cloned.1.call-done) | copy-start | bytes 12582916
  197.7 5.8 %copy-start.3 = (f32[256,2]{0,1:T(2,128)S(1)}, f32[256,2]{0,1:T(2,128)}, u32[]{:S(2)}) copy-start(f32[256,2]{0,1:T(2,128)} %param.9) | copy-start | bytes 6148
  199.7 28.8 %all-to-all-start.3 = ((bf16[2,512,512]{2,0,1:T(2,128)(2,1)}), bf16[2,512,512]{2,0,1:T(2,128)(2,1)S(1)}, u32[]{:S(2)}, u32[]{:S(2)}) async-start(bf16[2,512,512]{2,0,1:T(2,128)(2,1)} %copy.30), calls=%async_computation.3 | async-start | bytes 2097152 | tf_op jit(solution)/shard_map/all_to_all | solution.py:65
Sparse Core Ops, SparseCore 0:
  61.3 32.6 all-gather.2
  155.0 24.1 all-gather.4
